TPU v7x, 32 devices: a whole 2x2x4 slice. The times are simulated.
32 devices in a mesh: sp: 8 (over z, x), tp: 4 (over y, core).
Axes of the slice: x: 2, y: 2, z: 4, core: 2. Of those that a mesh axis runs over, the one named last changes fastest.
Arguments:
- residual: bfloat16 [6144, 2048], P('sp'), may hold values from -6 to 6
- queries: bfloat16 [6144, 1024], P('sp', 'tp'), may hold values from -12 to 12
- keys: bfloat16 [6144, 512], P('sp', 'tp'), may hold values from -6 to 6
- values: bfloat16 [6144, 512], P('sp', 'tp'), may hold values from -36 to 36
- segments: int32 [6144], P('sp'), may hold values from 0 to 3, never falling along the last dimension, each value on 1 to 3072 neighbouring positions
- sink: float32 [16], P('tp'), may hold values from 3 to 7
- out_weight: bfloat16 [1024, 2048], replicated, may hold values from -0.1875 to 0.1875
- norm_gain_one: float32 [2048], replicated, may hold values from 0.1 to 1.9
- group: int32 [6144], P('sp'), may hold values from 0 to 3, as said below
- member: int32 [6144, 2], P('sp'), may hold values from 0 to 7, as said below
- route_weight: float32 [6144, 2], P('sp'), may hold values from 0.25 to 1
- gate_weight: bfloat16 [32, 2048, 1024], P('sp', None, 'tp'), may hold values from -0.125 to 0.125
- up_weight: bfloat16 [32, 2048, 1024], P('sp', None, 'tp'), may hold values from -0.125 to 0.125
- down_weight: bfloat16 [32, 1024, 2048], P('sp', None, 'tp'), may hold values from -0.1875 to 0.1875
- norm_gain_two: float32 [2048], P('tp'), may hold values from 0.1 to 1.9
Outputs:
- output: bfloat16 [6144, 2048], P('sp', 'tp')
Inputs may be any that keep to these rules, and one draw needn't show every extreme that they name: In every aligned block of 192 rows no expert (group * 8 + member) is named by more than 24 rows, and one expert, the same in all blocks of a draw, is named by exactly 24 rows of every block. `member`: the 2 members of a row differ.
All inputs are finite; a program needn't handle non-finite values.
Results may differ from a plain program's by a relative error of at most 0.0059.
Values may be sent and summed in bfloat16 or wider, within the bound.
A program may use at most 128 MiB of HBM per device.

v0:
```python
import math

import jax
import jax.numpy as jnp
from jax import lax
from jax.sharding import PartitionSpec as P

HEAD_DIM = 64
HALF = 128
PER_GROUP = 8


ALPHA = 2.0**0.25
EPS = 1e-05


def with_halo(block, sides, width):
    for axis, dim in sides:
        count = lax.axis_size(axis)
        forward = [(i, i + 1) for i in range(count - 1)]
        backward = [(target, source) for source, target in forward]
        low = lax.ppermute(
            lax.slice_in_dim(block, block.shape[dim] - width, None, axis=dim), axis, forward
        )
        high = lax.ppermute(lax.slice_in_dim(block, 0, width, axis=dim), axis, backward)
        block = jnp.concatenate([low, block, high], axis=dim)
    return block


def layer_norm(summed, norm_gain):
    mean_value = jnp.mean(summed, -1, keepdims=True)
    variance = jnp.mean(jnp.square(summed - mean_value), -1, keepdims=True)
    return ((summed - mean_value) * lax.rsqrt(variance + EPS) * norm_gain).astype(jnp.bfloat16)


def shards(
    residual,
    queries,
    keys,
    values,
    segments,
    sink,
    out_weight,
    norm_gain_one,
    group,
    member,
    route_weight,
    gate_weight,
    up_weight,
    down_weight,
    norm_gain_two,
):
    row_count = queries.shape[0]
    sp_size = lax.axis_size("sp")
    tp_size = lax.axis_size("tp")
    kv_local = keys.shape[1] // HEAD_DIM
    heads_local = queries.shape[1] // HEAD_DIM
    group_size = heads_local // kv_local
    seq_total = row_count * sp_size
    seq_start = lax.axis_index("sp") * row_count
    joined = jnp.concatenate([keys, values], axis=1)
    padded, seg_padded = (
        with_halo(joined, (("sp", 0),), HALF),
        with_halo(segments, (("sp", 0),), HALF),
    )
    query_block = math.gcd(row_count, 512)
    key_span = query_block + 2 * HALF
    offsets = jnp.arange(key_span)[None, :] - HALF - jnp.arange(query_block)[:, None]
    in_band = jnp.abs(offsets) <= HALF
    sink_heads = sink.reshape(kv_local, group_size, 1, 1)
    query_heads = queries.reshape(row_count, kv_local, group_size, HEAD_DIM)
    key_cols = kv_local * HEAD_DIM
    pieces = []
    for number in range(row_count // query_block):
        row_low = number * query_block
        query_rows = query_heads[row_low : row_low + query_block]
        kv_rows = padded[row_low : row_low + key_span]
        key_part = kv_rows[:, :key_cols].reshape(key_span, kv_local, HEAD_DIM)
        value_part = kv_rows[:, key_cols:].reshape(key_span, kv_local, HEAD_DIM)
        key_place = seq_start + row_low - HALF + jnp.arange(key_span)
        inside = (key_place >= 0) & (key_place < seq_total)
        same_doc = (
            segments[row_low : row_low + query_block, None]
            == seg_padded[None, row_low : row_low + key_span]
        )
        allowed = in_band & same_doc & inside[None, :]
        scores = jnp.einsum(
            "qkgd,ckd->kgqc", query_rows, key_part, preferred_element_type=jnp.float32
        ) * HEAD_DIM ** (-0.5)
        masked = jnp.where(allowed, scores, -1e30)
        peak = jnp.maximum(jnp.max(masked, -1, keepdims=True), sink_heads)
        raised = jnp.where(allowed, jnp.exp(masked - peak), 0.0)
        denominator = jnp.sum(raised, -1, keepdims=True) + jnp.exp(sink_heads - peak)
        weights = (raised / denominator).astype(jnp.bfloat16)
        attended_part = jnp.einsum(
            "kgqc,ckd->qkgd", weights, value_part, preferred_element_type=jnp.float32
        )
        pieces.append(
            attended_part.reshape(query_block, heads_local * HEAD_DIM).astype(jnp.bfloat16)
        )
    attended = jnp.concatenate(pieces, 0)
    width = out_weight.shape[1]
    weight_rows = out_weight
    mixed = jnp.dot(
        lax.all_gather(attended, "tp", axis=1, tiled=True),
        weight_rows,
        preferred_element_type=jnp.float32,
    )
    pre_one = ALPHA * residual.astype(jnp.float32) + mixed
    normed = layer_norm(pre_one, norm_gain_one)
    experts_local = gate_weight.shape[0]
    expert_count = experts_local * sp_size
    picks_count = member.shape[1]
    block_rows = row_count // tp_size
    capacity = max(2, block_rows // 8)
    expert_ids = (group[:, None] * PER_GROUP + member).reshape(tp_size, block_rows * picks_count)
    onehot_table = (expert_ids[:, :, None] == jnp.arange(expert_count)[None, None, :]).astype(
        jnp.int32
    )
    ranks = jnp.sum((jnp.cumsum(onehot_table, 1) - 1) * onehot_table, 2)
    owner = expert_ids // experts_local
    local_ids = expert_ids % experts_local
    block_ids = jnp.arange(tp_size)[:, None]
    slot_all = ((local_ids * sp_size + owner) * tp_size + block_ids) * capacity + ranks
    copy_rows = (
        jnp.arange(row_count * picks_count).reshape(tp_size, block_rows * picks_count)
        // picks_count
    )
    extended = jnp.concatenate([normed, jnp.zeros((1, width), jnp.bfloat16)], 0)
    tp_place = lax.axis_index("tp")
    slot_own_base = (local_ids * sp_size + owner) * capacity + ranks
    own_slots = lax.dynamic_index_in_dim(slot_own_base, tp_place, 0, keepdims=False)
    own_rows = lax.dynamic_index_in_dim(copy_rows, tp_place, 0, keepdims=False)
    slot_count = experts_local * sp_size * capacity
    source = jnp.full((slot_count,), row_count, jnp.int32).at[own_slots].set(own_rows)
    outgoing = extended[source].reshape(experts_local, sp_size, capacity, width)
    received = lax.all_to_all(outgoing, "sp", split_axis=1, concat_axis=1, tiled=True)
    arrived = lax.all_gather(received, "tp", axis=2, tiled=True)
    expert_rows = arrived.reshape(experts_local, sp_size * tp_size * capacity, width)
    gate_part = jnp.einsum(
        "esd,edf->esf", expert_rows, gate_weight, preferred_element_type=jnp.float32
    )
    up_part = jnp.einsum("esd,edf->esf", expert_rows, up_weight, preferred_element_type=jnp.float32)
    hidden = (jax.nn.silu(gate_part) * up_part).astype(jnp.bfloat16)
    column_width = down_weight.shape[2]
    weight_rows = down_weight
    produced = jnp.einsum(
        "esf,efc->esc",
        lax.all_gather(hidden, "tp", axis=2, tiled=True),
        weight_rows,
        preferred_element_type=jnp.float32,
    ).astype(jnp.bfloat16)
    returned = lax.all_to_all(
        produced.reshape(experts_local, sp_size, tp_size * capacity, column_width),
        "sp",
        split_axis=1,
        concat_axis=1,
        tiled=True,
    )
    result_rows = returned.reshape(-1, column_width)
    picked = result_rows[slot_all.reshape(row_count, picks_count)]
    combined = jnp.sum(route_weight[:, :, None] * picked.astype(jnp.float32), 1)
    column_start = lax.axis_index("tp") * column_width
    normed_part = lax.dynamic_slice_in_dim(normed, column_start, column_width, 1)
    pre_two = ALPHA * normed_part.astype(jnp.float32) + combined
    sums, squares = lax.psum((jnp.sum(pre_two, -1), jnp.sum(pre_two * pre_two, -1)), "tp")
    mean_value = (sums / width)[:, None]
    variance = (squares / width)[:, None] - mean_value * mean_value
    return ((pre_two - mean_value) * lax.rsqrt(variance + EPS) * norm_gain_two).astype(jnp.bfloat16)


def solution(mesh):
    in_specs = (
        P("sp", None),
        P("sp", "tp"),
        P("sp", "tp"),
        P("sp", "tp"),
        P("sp"),
        P("tp"),
        P(),
        P(),
        P("sp"),
        P("sp", None),
        P("sp", None),
        P("sp", None, "tp"),
        P("sp", None, "tp"),
        P("sp", None, "tp"),
        P("tp"),
    )
    out_specs = P("sp", "tp")
    return jax.shard_map(shards, mesh=mesh, in_specs=in_specs, out_specs=out_specs, check_vma=False)
```

profile of v0, /device:TPU:0, one launch (start us, length us, event | category | flops | bytes accessed | tf_op | source)
XLA Modules:
  0.0 423.6 jit_solution(6903600422677034529)
XLA Ops:
  6.6 0.8 fusion.54
  7.4 4.9 %collective-permute-start.1 = (s32[128]{0:T(128)S(1)}, s32[128]{0:T(128)S(1)}, u32[]{:S(2)}, u32[]{:S(2)}) collective-permute-start(s32[128]{0:T(128)S(1)} %get-tuple-element.30), channel_id=1, source_target_pairs={{0,4},{4,8},{8,12},{12,16},{16,20},{20,24},{24,28},{1,5},{5,9},{9,... | collective-permute-start | bytes 1544 | tf_op jit(solution)/shard_map/ppermute | solution.py:22
  12.3 1.3 collective-permute-start.3
  13.6 1.0 constant_dynamic-update-slice_fusion.1
  14.5 1.0 constant_dynamic-update-slice_fusion
  15.5 0.6 fusion.52
  16.1 4.5 %collective-permute-start = (bf16[128,256]{1,0:T(8,128)(2,1)}, bf16[128,256]{1,0:T(8,128)(2,1)S(1)}, u32[]{:S(2)}, u32[]{:S(2)}) collective-permute-start(bf16[128,256]{1,0:T(8,128)(2,1)} %get-tuple-element.20), channel_id=1, source_target_pairs={{0,4},{4,8},{8,12},{12,16},{16,20},{20,24},{24,28},{1,5},{5,9},{9,... | collective-permute-start | bytes 196616 | tf_op jit(solution)/shard_map/ppermute | solution.py:22
  20.7 1.3 collective-permute-start.2
  22.0 0.7 slice.96
  22.7 0.8 fusion.55
  23.5 1.1 fusion.51
  24.8 0.8 copy.52
  26.0 0.7 and_and_fusion.2
  26.7 0.5 fusion.1
  27.2 0.6 copy-done.7
  27.9 1.5 pad_maximum_fusion.3
  29.4 1.0 copy.47
  30.4 0.8 copy.46
  31.4 0.5 fusion
  32.0 0.5 fusion.3
  32.6 0.5 fusion.2
  33.2 0.8 convolution_convert_fusion.3
  34.0 0.5 fusion.4
  34.5 0.5 fusion.5
  35.1 0.8 convolution_convert_fusion.2
  36.0 0.7 convolution_convert_fusion.1
  36.8 0.8 pad_maximum_fusion
  37.6 0.2 copy.59
  37.9 0.2 broadcast_add_fusion
  38.0 0.2 reshape.202
  38.3 0.3 eq.76
  38.5 3.5 reduce-window.6
  42.6 3.1 scatter_custom_fusion
  45.7 14.9 %all-gather.4.cloned.1.call-done = bf16[768,1024]{0,1:T(8,128)(2,1)} async-done(((bf16[768,256]{0,1:T(8,128)(2,1)}), bf16[768,1024]{0,1:T(8,128)(2,1)}) %all-gather.4.cloned.1.call-update) | async-done | bytes 1572880 | tf_op jit(solution)/shard_map/all_gather | solution.py:105
  60.6 7.8 %fusion.56 = (f32[768]{0:T(1024)S(1)}, f32[768,2048]{1,0:T(8,128)S(1)}) fusion(bf16[768,1024]{0,1:T(8,128)(2,1)} %all-gather.4.cloned.1.call-done, bf16[1024,2048]{1,0:T(8,128)(2,1)} %param.21, bf16[768,2048]{1,0:T(8,128)(2,1)} %param.15), kind=kOutput, calls=%fused_computation.146 | convolution fusion | flops 3227516160 | bytes 15207424 | tf_op jit(solution)/shard_map/dot_general | solution.py:104
  68.5 0.8 multiply_reduce_fusion
  69.3 0.9 multiply_convert_fusion
  70.1 1.7 copy-done
  71.8 0.2 concatenate.29
  72.0 4.3 %gather_fusion = bf16[768,2048]{1,0:T(8,128)(2,1)} fusion(bf16[769,2048]{1,0:T(8,128)(2,1)S(1)} %concatenate.29, s32[1024]{0:T(1024)S(1)} %pad_clamp_fusion.1), kind=kCustom, calls=%fused_computation | custom fusion | bytes 6294528 | tf_op jit(solution)/shard_map/gather | solution.py:136
  76.3 2.3 copy.63
  78.6 76.5 %all_to_all.10 = bf16[4,8,24,2048]{3,2,0,1:T(8,128)(2,1)} all-to-all(bf16[4,8,24,2048]{3,2,0,1:T(8,128)(2,1)S(1)} %copy.63), channel_id=1, replica_groups=mesh['sp'=8,'tp'=4] {'sp'}, dimensions={1} | all-to-all | bytes 6291456 | tf_op jit(solution)/shard_map/all_to_all | solution.py:137
  155.1 0.3 all-gather.8.cloned.1.call-start
  155.4 80.1 %all-gather.6.cloned.1.call-done = bf16[4,8,96,2048]{3,2,0,1:T(8,128)(2,1)} async-done(((bf16[4,8,24,2048]{3,2,0,1:T(8,128)(2,1)}), bf16[4,8,96,2048]{3,2,0,1:T(8,128)(2,1)}) %all-gather.6.cloned.1.call-update) | async-done | bytes 12582928 | tf_op jit(solution)/shard_map/all_gather | solution.py:138
  235.5 6.4 %copy.64 = bf16[4,8,96,2048]{3,2,1,0:T(8,128)(2,1)S(1)} copy(bf16[4,8,96,2048]{3,2,0,1:T(8,128)(2,1)} %all-gather.6.cloned.1.call-done) | data formatting | bytes 25165824 | tf_op jit(solution)/shard_map/all_gather | solution.py:138
  241.9 5.1 %fusion.57 = f32[4,768,256]{2,1,0:T(8,128)} fusion(bf16[4,768,2048]{2,1,0:T(8,128)(2,1)S(1)} %bitcast.120, bf16[4,2048,256]{2,1,0:T(8,128)(2,1)S(1)} %copy-done.14), kind=kOutput, calls=%fused_computation.147 | convolution fusion | flops 3221225472 | bytes 19922944 | tf_op jit(solution)/shard_map/esd,edf->esf/dot_general | solution.py:140
  247.1 7.4 %multiply_convert_fusion.1 = bf16[4,768,256]{2,1,0:T(8,128)(2,1)} fusion(f32[4,768,256]{2,1,0:T(8,128)} %fusion.57, bf16[4,768,2048]{2,1,0:T(8,128)(2,1)S(1)} %bitcast.121, bf16[4,2048,256]{2,1,0:T(8,128)(2,1)} %param.27), kind=kOutput, calls=%fused_computation.7 | convolution fusion | flops 3225944064 | bytes 21495808 | tf_op jit(solution)/shard_map/esd,edf->esf/dot_general | solution.py:143
  254.5 47.3 %all-gather.8.cloned.1.call-done = bf16[4,768,1024]{2,1,0:T(8,128)(2,1)} async-done(((bf16[4,768,256]{2,1,0:T(8,128)(2,1)}), bf16[4,768,1024]{2,1,0:T(8,128)(2,1)}) %all-gather.8.cloned.1.call-update) | async-done | bytes 6291472 | tf_op jit(solution)/shard_map/all_gather | solution.py:149
  301.8 7.4 %convolution_convert_fusion = bf16[4,768,512]{2,1,0:T(8,128)(2,1)S(1)} fusion(bf16[4,768,1024]{2,1,0:T(8,128)(2,1)} %all-gather.8.cloned.1.call-done, bf16[4,1024,512]{2,1,0:T(8,128)(2,1)} %param.28), kind=kOutput, calls=%fused_computation.8 | convolution fusion | flops 3222798336 | bytes 13631488 | tf_op jit(solution)/shard_map/esf,efc->esc/dot_general | solution.py:147
  309.3 2.0 copy.65
  311.3 5.7 %all-to-all-start.1 = ((bf16[4,8,96,512]{3,2,0,1:T(8,128)(2,1)}), bf16[4,8,96,512]{3,2,0,1:T(8,128)(2,1)}, u32[]{:S(2)}, u32[]{:S(2)}) async-start(bf16[4,8,96,512]{3,2,0,1:T(8,128)(2,1)} %copy.65), calls=%async_computation.1 | async-start | bytes 6291456 | tf_op jit(solution)/shard_map/all_to_all | solution.py:153
  316.9 0.3 reduce_sum.89
  317.4 0.5 compare_select_fusion
  317.9 0.2 reshape.221
  318.1 0.2 copy.58
  318.3 69.8 %all-to-all-done.1 = bf16[4,8,96,512]{3,2,0,1:T(8,128)(2,1)} async-done(((bf16[4,8,96,512]{3,2,0,1:T(8,128)(2,1)}), bf16[4,8,96,512]{3,2,0,1:T(8,128)(2,1)}, u32[]{:S(2)}, u32[]{:S(2)}) %all-to-all-start.1) | async-done | bytes 3145760 | tf_op jit(solution)/shard_map/all_to_all | solution.py:153
  388.1 2.2 copy.66
  390.4 5.4 %gather_fusion.1 = bf16[1536,512]{1,0:T(8,128)(2,1)} fusion(bf16[3072,512]{1,0:T(8,128)(2,1)S(1)} %bitcast.119, s32[2048]{0:T(1024)S(1)} %pad_clamp_fusion), kind=kCustom, calls=%fused_computation.1 | custom fusion | bytes 3151872 | tf_op jit(solution)/shard_map/gather | solution.py:161
  395.8 4.8 %reshape.238 = f32[768,2,512]{2,1,0:T(2,128)} reshape(bf16[1536,512]{1,0:T(8,128)(2,1)} %gather_fusion.1) | data formatting | bytes 4718592 | tf_op jit(solution)/shard_map/convert_element_type | solution.py:162
  400.6 6.1 %multiply_reduce_fusion.1 = f32[768,512]{1,0:T(8,128)S(1)} fusion(f32[768,2,512]{2,1,0:T(2,128)} %reshape.238, f32[768,2]{1,0:T(8,128)S(1)} %copy.58), kind=kLoop, calls=%fused_computation.6 | loop fusion | flops 1179648 | bytes 4724736 | tf_op jit(solution)/shard_map/reduce_sum | solution.py:162
  406.7 1.2 copy-done.2
  407.9 0.4 fusion.16
  408.3 6.1 %all-reduce.1 = (f32[768]{0:T(1024)S(1)}, f32[768]{0:T(1024)S(1)}) all-reduce(f32[768]{0:T(1024)S(1)} %get-tuple-element.6, f32[768]{0:T(1024)S(1)} %get-tuple-element.5), channel_id=1, replica_groups=mesh['sp'=8,'tp'=4] {'tp'}, use_global_device_ids=true, to_apply=%region_16.17 | all-reduce | flops 1536 | bytes 12288 | tf_op jit(solution)/shard_map/psum | solution.py:166
  414.4 2.6 multiply_convert_fusion.2
  (81 shorter events, 2.0 us)
Async XLA Ops:
  6.5 19.4 %copy-start.8 = (s32[768]{0:T(1024)S(1)}, s32[768]{0:T(1024)}, u32[]{:S(2)}) copy-start(s32[768]{0:T(1024)} %param.19) | copy-start | bytes 9220
  6.5 18.1 %slice-start = ((bf16[768,128]{1,0:T(8,128)(2,1)}), bf16[512,128]{1,0:T(8,128)(2,1)S(1)}, s32[]{:S(2)}) async-start(bf16[768,128]{1,0:T(8,128)(2,1)} %param.17), calls=%async_computation.5 | async-start | bytes 262144 | tf_op jit(solution)/shard_map/slice | solution.py:78
  6.5 18.3 %slice-start.1 = ((bf16[768,128]{1,0:T(8,128)(2,1)}), bf16[512,128]{1,0:T(8,128)(2,1)S(1)}, s32[]{:S(2)}) async-start(bf16[768,128]{1,0:T(8,128)(2,1)} %param.18), calls=%async_computation.6 | async-start | bytes 262144 | tf_op jit(solution)/shard_map/slice | solution.py:79
  6.5 18.0 %copy-start.15 = (f32[4]{0:T(128)S(1)}, f32[4]{0:T(128)}, u32[]{:S(2)}) copy-start(f32[4]{0:T(128)} %param.20) | copy-start | bytes 52
  6.5 54.1 %all-gather.4.cloned.1.call-start = ((), (), s32[]{:S(2)}) async-start(), calls=%async_computation.2 | async-start | bytes 1966080 | tf_op jit(solution)/shard_map/all_gather | solution.py:105
  7.4 18.5 %collective-permute-start.1 = (s32[128]{0:T(128)S(1)}, s32[128]{0:T(128)S(1)}, u32[]{:S(2)}, u32[]{:S(2)}) collective-permute-start(s32[128]{0:T(128)S(1)} %get-tuple-element.30), channel_id=1, source_target_pairs={{0,4},{4,8},{8,12},{12,16},{16,20},{20,24},{24,28},{1,5},{5,9},{9,... | collective-permute-start | bytes 1544 | tf_op jit(solution)/shard_map/ppermute | solution.py:22
  12.3 13.6 %collective-permute-start.3 = (s32[128]{0:T(128)S(1)}, s32[128]{0:T(128)S(1)}, u32[]{:S(2)}, u32[]{:S(2)}) collective-permute-start(s32[128]{0:T(128)S(1)} %get-tuple-element.31), channel_id=1, source_target_pairs={{4,0},{8,4},{12,8},{16,12},{20,16},{24,20},{28,24},{5,1},{9,5},{13... | collective-permute-start | bytes 1544 | tf_op jit(solution)/shard_map/ppermute | solution.py:25
  16.1 11.1 %collective-permute-start = (bf16[128,256]{1,0:T(8,128)(2,1)}, bf16[128,256]{1,0:T(8,128)(2,1)S(1)}, u32[]{:S(2)}, u32[]{:S(2)}) collective-permute-start(bf16[128,256]{1,0:T(8,128)(2,1)} %get-tuple-element.20), channel_id=1, source_target_pairs={{0,4},{4,8},{8,12},{12,16},{16,20},{20,24},{24,28},{1,5},{5,9},{9,... | collective-permute-start | bytes 196616 | tf_op jit(solution)/shard_map/ppermute | solution.py:22
  20.7 7.2 %collective-permute-start.2 = (bf16[128,256]{1,0:T(8,128)(2,1)S(1)}, bf16[128,256]{1,0:T(8,128)(2,1)}, u32[]{:S(2)}, u32[]{:S(2)}) collective-permute-start(bf16[128,256]{1,0:T(8,128)(2,1)S(1)} %get-tuple-element.21), channel_id=1, source_target_pairs={{4,0},{8,4},{12,8},{16,12},{20,16},{24,20},{28,24},{5,1},{9,5},{13... | collective-permute-start | bytes 196616 | tf_op jit(solution)/shard_map/ppermute | solution.py:25
  27.2 0.6 copy-start.7
  32.0 1.2 copy-start.6
  35.1 0.9 copy-start.5
  36.0 1.6 copy-start.10
  36.0 1.8 copy-start.12
  37.6 197.9 %all-gather.6.cloned.1.call-start = ((), (), s32[]{:S(2)}) async-start(), calls=%async_computation.3 | async-start | bytes 15728640 | tf_op jit(solution)/shard_map/all_gather | solution.py:138
  37.8 30.6 %copy-start.3 = (s32[768,2]{1,0:T(8,128)}, s32[768,2]{1,0:T(8,128)S(1)}, u32[]{:S(2)}) copy-start(s32[768,2]{1,0:T(8,128)S(1)} %copy.59) | copy-start | bytes 18436
  68.5 0.8 copy-start.9
  70.1 1.7 copy-start
  155.1 146.7 %all-gather.8.cloned.1.call-start = ((), (), s32[]{:S(2)}) async-start(), calls=%async_computation.4 | async-start | bytes 7864320 | tf_op jit(solution)/shard_map/all_gather | solution.py:149
  235.5 6.5 %copy-start.14 = (bf16[4,2048,256]{2,1,0:T(8,128)(2,1)S(1)}, bf16[4,2048,256]{2,1,0:T(8,128)(2,1)}, u32[]{:S(2)}) copy-start(bf16[4,2048,256]{2,1,0:T(8,128)(2,1)} %param.26) | copy-start | bytes 12582916
  311.3 6.1 %copy-start.4 = (s32[768,2]{1,0:T(8,128)S(1)}, s32[768,2]{1,0:T(8,128)}, u32[]{:S(2)}) copy-start(s32[768,2]{1,0:T(8,128)} %copy-done.3) | copy-start | bytes 18436
  311.3 6.9 %copy-start.11 = (f32[768,2]{0,1:T(2,128)S(1)}, f32[768,2]{0,1:T(2,128)}, u32[]{:S(2)}) copy-start(f32[768,2]{0,1:T(2,128)} %param.25) | copy-start | bytes 18436
  311.3 76.9 %all-to-all-start.1 = ((bf16[4,8,96,512]{3,2,0,1:T(8,128)(2,1)}), bf16[4,8,96,512]{3,2,0,1:T(8,128)(2,1)}, u32[]{:S(2)}, u32[]{:S(2)}) async-start(bf16[4,8,96,512]{3,2,0,1:T(8,128)(2,1)} %copy.65), calls=%async_computation.1 | async-start | bytes 6291456 | tf_op jit(solution)/shard_map/all_to_all | solution.py:153
  400.6 7.3 %copy-start.1 = (bf16[768,2048]{1,0:T(8,128)(2,1)S(1)}, bf16[768,2048]{1,0:T(8,128)(2,1)}, u32[]{:S(2)}) copy-start(bf16[768,2048]{1,0:T(8,128)(2,1)} %copy-done) | copy-start | bytes 9437188
  406.7 1.2 copy-start.2
  407.9 6.5 %copy-start.13 = (f32[512]{0:T(512)S(1)}, f32[512]{0:T(512)}, u32[]{:S(2)}) copy-start(f32[512]{0:T(512)} %param.29) | copy-start | bytes 6148
Sparse Core Ops, SparseCore 0:
  37.7 22.9 all-gather.3
  155.2 80.1 all-gather.5
  254.6 47.1 all-gather.7
where the time goes:
time: 424 us
  waiting for transfers between devices  212 us (50%)
  blocking collectives  82.6 us (19%)
  local copies, waits for them, and re-layouts  45.3 us (11%)
  matrix products  31.6 us (7%)
  other arithmetic  20.2 us (5%)
  starting transfers between devices  18 us (4%)
  between operations  13.7 us (3%)
    all_gather x1, waiting for transfers between devices, shards(): arrived = lax.all_gather(received, 'tp', axis=2, tiled=True)  80.1 us
    all_to_all x1, blocking collectives, shards(): lax.all_to_all(outgoing, 'sp', split_axis=1, concat_axis=1, tiled=True)  76.5 us
    all_to_all x1, waiting for transfers between devices, shards(): lax.all_to_all(produced.reshape(experts_local, sp_size, tp_size * capacit...  69.8 us
    all_gather x1, waiting for transfers between devices, shards(): lax.all_gather(hidden, 'tp', axis=2, tiled=True)  47.3 us
    all_gather x1, waiting for transfers between devices, shards(): lax.all_gather(attended, 'tp', axis=1, tiled=True)  14.9 us
    ppermute x2, starting transfers between devices, with_halo(): lax.ppermute(lax.slice_in_dim(block, block.shape[dim] - width, None, axis...  9.4 us
  transfers between devices with their start and end apart: 8, of which 4 were waited for; matrix products, arithmetic and copies ran while one was open for 4% of the time, Pallas kernels for 0%

commit v1 on v0

--- a/solution.py
+++ b/solution.py
@@ -1,8 +1,11 @@
+import functools
 import math
 
 import jax
 import jax.numpy as jnp
 from jax import lax
+from jax.experimental import pallas as pl
+from jax.experimental.pallas import tpu as pltpu
 from jax.sharding import PartitionSpec as P
 
 HEAD_DIM = 64
@@ -31,6 +34,335 @@
     mean_value = jnp.mean(summed, -1, keepdims=True)
     variance = jnp.mean(jnp.square(summed - mean_value), -1, keepdims=True)
     return ((summed - mean_value) * lax.rsqrt(variance + EPS) * norm_gain).astype(jnp.bfloat16)
+
+
+MESH = pl.DeviceIdType.MESH
+
+
+def expert_kernel(
+    groups,
+    out_ref,
+    pick_ref,
+    join_ref,
+    gate_hbm,
+    up_hbm,
+    down_hbm,
+    result_ref,
+    rows,
+    taken,
+    gate,
+    up,
+    down,
+    hidden,
+    made,
+    kept,
+    across,
+    beside,
+    summed,
+    back,
+    weight_sem,
+    place_sem,
+    send_sem,
+    recv_sem,
+):
+    sp = lax.axis_index("sp")
+    tp = lax.axis_index("tp")
+    z, x = sp // 2, sp % 2
+    y, c = tp // 2, tp % 2
+    room = out_ref.shape[1]
+    experts = gate.shape[0]
+    first = room // 2 // 16 * 16
+
+    load_gate = pltpu.make_async_copy(gate_hbm, gate, weight_sem.at[0])
+    load_up = pltpu.make_async_copy(up_hbm, up, weight_sem.at[1])
+    load_down = pltpu.make_async_copy(down_hbm, down, weight_sem.at[2])
+    load_gate.start()
+    load_up.start()
+    load_down.start()
+
+    beside_x = (z * 2 + 1 - x, tp)
+    beside_y = (sp, (1 - y) * 2 + c)
+    sibling = (sp, y * 2 + 1 - c)
+    far = [(lax.rem(z + k, groups) * 2 + x, tp) for k in range(1, groups)]
+    barrier = pltpu.get_barrier_semaphore()
+    for device in [beside_x, beside_y, sibling] + far:
+        pl.semaphore_signal(barrier, inc=1, device_id=device, device_id_type=MESH)
+    pl.semaphore_wait(barrier, groups + 2)
+
+    def place(zs, xs, ys, cs, low=0, size=None):
+        size = room if size is None else size
+        start = pl.multiple_of(cs * room + low, 16)
+        return rows.at[(zs * 2 + xs) * 2 + ys, pl.ds(start, size)]
+
+    def copy(ref, device, kind, k, source=None):
+        return pltpu.make_async_remote_copy(
+            src_ref=ref if source is None else source,
+            dst_ref=ref,
+            send_sem=send_sem.at[kind, k],
+            recv_sem=recv_sem.at[kind, k],
+            device_id=device,
+            device_id_type=MESH,
+        )
+
+    started = []
+
+    def send(*args, **named):
+        one = copy(*args, **named)
+        one.start()
+        started.append(one)
+
+    def arrive(ref, kind, k):
+        copy(ref, sibling, kind, k).wait_recv()
+
+    own = pltpu.make_async_copy(out_ref.at[z], place(z, x, y, c), place_sem)
+    own.start()
+    for k in range(1, groups):
+        send(place(z, x, y, c), far[k - 1], 0, k, source=out_ref.at[lax.rem(z + k, groups)])
+    own.wait()
+    sources = [lax.rem(z + groups - k, groups) for k in range(groups)]
+
+    def begin(k):
+        zs = sources[k]
+        if k:
+            arrive(place(zs, x, y, c), 0, k)
+        send(place(zs, x, y, c), beside_x, 1, k)
+        send(place(zs, x, y, c), beside_y, 2, k)
+        send(place(zs, x, y, c), sibling, 3, k)
+
+    def forward(k):
+        zs = sources[k]
+        arrive(place(zs, 1 - x, y, c), 1, k)
+        send(place(zs, 1 - x, y, c, 0, first), beside_y, 4, k)
+        send(place(zs, 1 - x, y, c), sibling, 6, k)
+        arrive(place(zs, x, 1 - y, c), 2, k)
+        send(place(zs, x, 1 - y, c, first, room - first), beside_x, 5, k)
+        send(place(zs, x, 1 - y, c), sibling, 7, k)
+
+    def finish(k):
+        zs = sources[k]
+        arrive(place(zs, 1 - x, 1 - y, c, 0, first), 4, k)
+        send(place(zs, 1 - x, 1 - y, c, 0, first), sibling, 8, k)
+        arrive(place(zs, 1 - x, 1 - y, c, first, room - first), 5, k)
+        send(place(zs, 1 - x, 1 - y, c, first, room - first), sibling, 9, k)
+        arrive(place(zs, x, y, 1 - c), 3, k)
+        arrive(place(zs, 1 - x, y, 1 - c), 6, k)
+        arrive(place(zs, x, 1 - y, 1 - c), 7, k)
+        arrive(place(zs, 1 - x, 1 - y, 1 - c, 0, first), 8, k)
+        arrive(place(zs, 1 - x, 1 - y, 1 - c, first, room - first), 9, k)
+
+    pair_rows = pick_ref.shape[1] // experts
+
+    def compute(k):
+        zs = sources[k]
+        for pair in range(4):
+            chosen = jnp.dot(
+                pick_ref[zs * 4 + pair], rows[zs * 4 + pair], preferred_element_type=jnp.float32
+            ).astype(jnp.bfloat16)
+            for e in range(experts):
+                taken[e, pair * pair_rows : (pair + 1) * pair_rows, :] = chosen[
+                    e * pair_rows : (e + 1) * pair_rows
+                ]
+
+        def one(e, carry):
+            gate_part = jnp.dot(taken[e], gate[e], preferred_element_type=jnp.float32)
+            up_part = jnp.dot(taken[e], up[e], preferred_element_type=jnp.float32)
+            silu = gate_part / (1.0 + jnp.exp(-gate_part))
+            hidden[zs, tp, e] = (silu * up_part).astype(jnp.bfloat16)
+            return carry
+
+        lax.fori_loop(0, experts, one, 0)
+        send(hidden.at[zs, tp], beside_y, 10, k)
+        send(hidden.at[zs, tp], sibling, 11, k)
+
+    def share(k):
+        other = hidden.at[sources[k], (1 - y) * 2 + c]
+        arrive(other, 10, k)
+        send(other, sibling, 12, k)
+
+    part = down.shape[1] // 4
+
+    def project(k):
+        zs = sources[k]
+        arrive(hidden.at[zs, y * 2 + 1 - c], 11, k)
+        arrive(hidden.at[zs, (1 - y) * 2 + 1 - c], 12, k)
+        if k == 0:
+            load_down.wait()
+
+        def one(e, carry):
+            total = jnp.dot(
+                hidden[zs, 0, e], down[e, :part, :], preferred_element_type=jnp.float32
+            )
+            for t in range(1, 4):
+                total += jnp.dot(
+                    hidden[zs, t, e],
+                    down[e, t * part : (t + 1) * part, :],
+                    preferred_element_type=jnp.float32,
+                )
+            total = total.astype(jnp.bfloat16)
+            start = pl.multiple_of(e * pair_rows, 16)
+            for pair in range(4):
+                made[pair, pl.ds(start, pair_rows), :] = total[
+                    pair * pair_rows : (pair + 1) * pair_rows
+                ]
+            return carry
+
+        lax.fori_loop(0, experts, one, 0)
+
+        def joined(xs, ys):
+            at = zs * 4 + xs * 2 + ys
+            slots = made[xs * 2 + ys]
+            return jnp.dot(
+                join_ref[0, at], slots, preferred_element_type=jnp.float32
+            ) + jnp.dot(join_ref[1, at], slots, preferred_element_type=jnp.float32)
+
+        for ys in range(2):
+            across[zs, ys] = joined(1 - x, ys).astype(jnp.bfloat16)
+        send(beside.at[zs], beside_x, 13, k, source=across.at[zs])
+        for ys in range(2):
+            kept[k % 2, ys] = joined(x, ys)
+
+    def give(k):
+        zs = sources[k]
+        arrive(beside.at[zs], 13, k)
+        total = (kept[k % 2] + beside[zs].astype(jnp.float32)).astype(jnp.bfloat16)
+        if k == 0:
+            back[z] = total
+        else:
+            summed[k] = total
+            send(back.at[z], (zs * 2 + x, tp), 14, k, source=summed.at[k])
+
+    for k in range(groups + 3):
+        if k < groups:
+            begin(k)
+        if 0 < k <= groups:
+            finish(k - 1)
+            if k == 1:
+                load_gate.wait()
+                load_up.wait()
+            compute(k - 1)
+        if k < groups:
+            forward(k)
+        if 0 < k <= groups:
+            share(k - 1)
+        if 0 <= k - 2 < groups:
+            project(k - 2)
+        if 0 <= k - 3 < groups:
+            give(k - 3)
+    for k in range(1, groups):
+        arrive(back.at[lax.rem(z + k, groups)], 14, k)
+    result_ref[...] = back[...]
+    for one in started:
+        one.wait_send()
+
+
+def group_experts(outgoing, picks, joins, gate_weight, up_weight, down_weight):
+    groups, room, width = outgoing.shape
+    experts, _, hidden_width = gate_weight.shape
+    pairs, pair_slots, pair_rows = picks.shape
+    chunk = pair_slots // experts * 4
+    out_width = down_weight.shape[2]
+    part = (groups, 2, pair_rows, out_width)
+    return pl.pallas_call(
+        functools.partial(expert_kernel, groups),
+        out_shape=jax.ShapeDtypeStruct(part, jnp.bfloat16),
+        in_specs=[
+            pl.BlockSpec(memory_space=pltpu.VMEM),
+            pl.BlockSpec(memory_space=pltpu.VMEM),
+            pl.BlockSpec(memory_space=pltpu.VMEM),
+            pl.BlockSpec(memory_space=pl.ANY),
+            pl.BlockSpec(memory_space=pl.ANY),
+            pl.BlockSpec(memory_space=pl.ANY),
+        ],
+        out_specs=pl.BlockSpec(memory_space=pltpu.VMEM),
+        scratch_shapes=[
+            pltpu.VMEM((pairs, pair_rows, width), jnp.bfloat16),
+            pltpu.VMEM((experts, chunk, width), jnp.bfloat16),
+            pltpu.VMEM(gate_weight.shape, jnp.bfloat16),
+            pltpu.VMEM(up_weight.shape, jnp.bfloat16),
+            pltpu.VMEM(down_weight.shape, jnp.bfloat16),
+            pltpu.VMEM((groups, 4, experts, chunk, hidden_width), jnp.bfloat16),
+            pltpu.VMEM((4, pair_slots, out_width), jnp.bfloat16),
+            pltpu.VMEM((2,) + part[1:], jnp.float32),
+            pltpu.VMEM(part, jnp.bfloat16),
+            pltpu.VMEM(part, jnp.bfloat16),
+            pltpu.VMEM(part, jnp.bfloat16),
+            pltpu.VMEM(part, jnp.bfloat16),
+            pltpu.SemaphoreType.DMA((3,)),
+            pltpu.SemaphoreType.DMA,
+            pltpu.SemaphoreType.DMA((15, groups)),
+            pltpu.SemaphoreType.DMA((15, groups)),
+        ],
+        compiler_params=pltpu.CompilerParams(
+            collective_id=0, has_side_effects=True, vmem_limit_bytes=63 * 1024 * 1024
+        ),
+    )(outgoing, picks, joins, gate_weight, up_weight, down_weight)
+
+
+def group_ranks(mine):
+    count = mine.astype(jnp.int32)
+    return jnp.cumsum(count, 1) - count
+
+
+def experts_by_group(
+    normed, group, member, route_weight, gate_weight, up_weight, down_weight, capacity
+):
+    sp_size, tp_size = lax.axis_size("sp"), lax.axis_size("tp")
+    row_count = normed.shape[0]
+    block_rows = row_count // tp_size
+    experts_local = gate_weight.shape[0]
+    groups = experts_local * sp_size // PER_GROUP
+    room = capacity * PER_GROUP // member.shape[1]
+    packed = (group * PER_GROUP + member[:, 0]) * PER_GROUP + member[:, 1]
+    every = lax.all_gather(packed, "sp", axis=0, tiled=True).reshape(-1, block_rows)
+    own_group = lax.axis_index("sp") * experts_local // PER_GROUP
+    first_expert = lax.axis_index("sp") * experts_local % PER_GROUP
+    mine = every // (PER_GROUP * PER_GROUP) == own_group
+    at = group_ranks(mine)
+    names = [every // PER_GROUP % PER_GROUP, every % PER_GROUP]
+    local = first_expert + jnp.arange(experts_local)[None, :, None]
+    named = ((names[0][:, None, :] == local) | (names[1][:, None, :] == local)) & mine[:, None, :]
+    slot = jnp.cumsum(named.astype(jnp.int32), 2) - 1
+    slot = jnp.where(named, slot, -1)
+    blocks = every.shape[0]
+    slot_hot = (slot[:, :, None, :] == jnp.arange(capacity)[None, None, :, None]).astype(jnp.bfloat16)
+    row_hot = (
+        (at[:, :, None] == jnp.arange(room)[None, None, :]) & mine[:, :, None]
+    ).astype(jnp.bfloat16)
+    pick = jnp.einsum(
+        "bsr,brg->bsg",
+        slot_hot.reshape(blocks, experts_local * capacity, block_rows),
+        row_hot,
+        preferred_element_type=jnp.float32,
+    ).astype(jnp.bfloat16)
+    pick = pick.reshape(blocks // 2, 2, experts_local, capacity, room).transpose(0, 2, 1, 3, 4)
+    both = jnp.eye(2, dtype=jnp.bfloat16)[None, None, :, None, :, None] * pick[:, :, :, :, None, :]
+    picks = both.reshape(blocks // 2, experts_local * 2 * capacity, 2 * room)
+    routes = lax.all_gather(route_weight.T, "sp", axis=1, tiled=True)
+    routes = routes.reshape(2, blocks, 1, block_rows)
+    routed = jnp.where(names[0][:, None, :] == local, routes[0], routes[1])
+    slot_weight = jnp.sum(slot_hot.astype(jnp.float32) * routed[:, :, None, :], 3)
+    slot_weight = slot_weight.reshape(blocks // 2, 2, experts_local, capacity)
+    slot_weight = slot_weight.transpose(0, 2, 1, 3).reshape(blocks // 2, 1, -1)
+    coarse = slot_weight.astype(jnp.bfloat16)
+    fine = (slot_weight - coarse.astype(jnp.float32)).astype(jnp.bfloat16)
+    joins = picks.transpose(0, 2, 1)[None] * jnp.stack([coarse, fine])
+    by_block = group.reshape(tp_size, block_rows)
+    group_mask = by_block[:, None, :] == jnp.arange(groups)[None, :, None]
+    count = group_mask.astype(jnp.int32)
+    place = jnp.cumsum(count, 2) - count
+    choose = (
+        (place[:, :, None, :] == jnp.arange(room)[None, None, :, None]) & group_mask[:, :, None, :]
+    ).astype(jnp.bfloat16)
+    choose = choose.reshape(tp_size, groups * room, block_rows)
+    own_choose = lax.dynamic_index_in_dim(choose, lax.axis_index("tp"), 0, keepdims=False)
+    own_rows = lax.dynamic_slice_in_dim(normed, lax.axis_index("tp") * block_rows, block_rows, 0)
+    outgoing = jnp.dot(own_choose, own_rows, preferred_element_type=jnp.float32)
+    outgoing = outgoing.astype(jnp.bfloat16).reshape(groups, room, normed.shape[1])
+    back = group_experts(outgoing, picks, joins, gate_weight, up_weight, down_weight)
+    back = back.reshape(groups, tp_size, room, -1).transpose(1, 0, 2, 3)
+    back = back.reshape(tp_size, groups * room, -1)
+    combined = jnp.einsum("tgr,tgc->trc", choose, back, preferred_element_type=jnp.float32)
+    return combined.reshape(row_count, -1)
 
 
 def shards(
@@ -113,53 +445,58 @@
     picks_count = member.shape[1]
     block_rows = row_count // tp_size
     capacity = max(2, block_rows // 8)
-    expert_ids = (group[:, None] * PER_GROUP + member).reshape(tp_size, block_rows * picks_count)
-    onehot_table = (expert_ids[:, :, None] == jnp.arange(expert_count)[None, None, :]).astype(
-        jnp.int32
-    )
-    ranks = jnp.sum((jnp.cumsum(onehot_table, 1) - 1) * onehot_table, 2)
-    owner = expert_ids // experts_local
-    local_ids = expert_ids % experts_local
-    block_ids = jnp.arange(tp_size)[:, None]
-    slot_all = ((local_ids * sp_size + owner) * tp_size + block_ids) * capacity + ranks
-    copy_rows = (
-        jnp.arange(row_count * picks_count).reshape(tp_size, block_rows * picks_count)
-        // picks_count
-    )
-    extended = jnp.concatenate([normed, jnp.zeros((1, width), jnp.bfloat16)], 0)
-    tp_place = lax.axis_index("tp")
-    slot_own_base = (local_ids * sp_size + owner) * capacity + ranks
-    own_slots = lax.dynamic_index_in_dim(slot_own_base, tp_place, 0, keepdims=False)
-    own_rows = lax.dynamic_index_in_dim(copy_rows, tp_place, 0, keepdims=False)
-    slot_count = experts_local * sp_size * capacity
-    source = jnp.full((slot_count,), row_count, jnp.int32).at[own_slots].set(own_rows)
-    outgoing = extended[source].reshape(experts_local, sp_size, capacity, width)
-    received = lax.all_to_all(outgoing, "sp", split_axis=1, concat_axis=1, tiled=True)
-    arrived = lax.all_gather(received, "tp", axis=2, tiled=True)
-    expert_rows = arrived.reshape(experts_local, sp_size * tp_size * capacity, width)
-    gate_part = jnp.einsum(
-        "esd,edf->esf", expert_rows, gate_weight, preferred_element_type=jnp.float32
-    )
-    up_part = jnp.einsum("esd,edf->esf", expert_rows, up_weight, preferred_element_type=jnp.float32)
-    hidden = (jax.nn.silu(gate_part) * up_part).astype(jnp.bfloat16)
     column_width = down_weight.shape[2]
-    weight_rows = down_weight
-    produced = jnp.einsum(
-        "esf,efc->esc",
-        lax.all_gather(hidden, "tp", axis=2, tiled=True),
-        weight_rows,
-        preferred_element_type=jnp.float32,
-    ).astype(jnp.bfloat16)
-    returned = lax.all_to_all(
-        produced.reshape(experts_local, sp_size, tp_size * capacity, column_width),
-        "sp",
-        split_axis=1,
-        concat_axis=1,
-        tiled=True,
-    )
-    result_rows = returned.reshape(-1, column_width)
-    picked = result_rows[slot_all.reshape(row_count, picks_count)]
-    combined = jnp.sum(route_weight[:, :, None] * picked.astype(jnp.float32), 1)
+    if experts_local * 2 == PER_GROUP and tp_size == 4:
+        combined = experts_by_group(
+            normed, group, member, route_weight, gate_weight, up_weight, down_weight, capacity
+        )
+    else:
+        expert_ids = (group[:, None] * PER_GROUP + member).reshape(tp_size, block_rows * picks_count)
+        onehot_table = (expert_ids[:, :, None] == jnp.arange(expert_count)[None, None, :]).astype(
+            jnp.int32
+        )
+        ranks = jnp.sum((jnp.cumsum(onehot_table, 1) - 1) * onehot_table, 2)
+        owner = expert_ids // experts_local
+        local_ids = expert_ids % experts_local
+        block_ids = jnp.arange(tp_size)[:, None]
+        slot_all = ((local_ids * sp_size + owner) * tp_size + block_ids) * capacity + ranks
+        copy_rows = (
+            jnp.arange(row_count * picks_count).reshape(tp_size, block_rows * picks_count)
+            // picks_count
+        )
+        extended = jnp.concatenate([normed, jnp.zeros((1, width), jnp.bfloat16)], 0)
+        tp_place = lax.axis_index("tp")
+        slot_own_base = (local_ids * sp_size + owner) * capacity + ranks
+        own_slots = lax.dynamic_index_in_dim(slot_own_base, tp_place, 0, keepdims=False)
+        own_rows = lax.dynamic_index_in_dim(copy_rows, tp_place, 0, keepdims=False)
+        slot_count = experts_local * sp_size * capacity
+        source = jnp.full((slot_count,), row_count, jnp.int32).at[own_slots].set(own_rows)
+        outgoing = extended[source].reshape(experts_local, sp_size, capacity, width)
+        received = lax.all_to_all(outgoing, "sp", split_axis=1, concat_axis=1, tiled=True)
+        arrived = lax.all_gather(received, "tp", axis=2, tiled=True)
+        expert_rows = arrived.reshape(experts_local, sp_size * tp_size * capacity, width)
+        gate_part = jnp.einsum(
+            "esd,edf->esf", expert_rows, gate_weight, preferred_element_type=jnp.float32
+        )
+        up_part = jnp.einsum("esd,edf->esf", expert_rows, up_weight, preferred_element_type=jnp.float32)
+        hidden = (jax.nn.silu(gate_part) * up_part).astype(jnp.bfloat16)
+        weight_rows = down_weight
+        produced = jnp.einsum(
+            "esf,efc->esc",
+            lax.all_gather(hidden, "tp", axis=2, tiled=True),
+            weight_rows,
+            preferred_element_type=jnp.float32,
+        ).astype(jnp.bfloat16)
+        returned = lax.all_to_all(
+            produced.reshape(experts_local, sp_size, tp_size * capacity, column_width),
+            "sp",
+            split_axis=1,
+            concat_axis=1,
+            tiled=True,
+        )
+        result_rows = returned.reshape(-1, column_width)
+        picked = result_rows[slot_all.reshape(row_count, picks_count)]
+        combined = jnp.sum(route_weight[:, :, None] * picked.astype(jnp.float32), 1)
     column_start = lax.axis_index("tp") * column_width
     normed_part = lax.dynamic_slice_in_dim(normed, column_start, column_width, 1)
     pre_two = ALPHA * normed_part.astype(jnp.float32) + combined

time: 424 us -> 321 us (0.76)
  waiting for transfers between devices: 212 us -> 0.03 us
  Pallas kernels: 0 us -> 151 us
  local copies, waits for them, and re-layouts: 45.3 us -> 28.5 us
  matrix products: 31.6 us -> 16.1 us
  blocking collectives: 82.6 us -> 69.7 us
  other arithmetic: 20.2 us -> 27.6 us
  starting transfers between devices: 18 us -> 13.1 us
    pallas_call x0 -> x1, Pallas kernels: none -> 151 us  [group_experts(): pl.pallas_call(functools.partial(expert_kernel, groups), out_shape=jax.Sh...]
    all_gather x2 -> x0, waiting for transfers between devices: 127 us -> none  [the longest x1 80.1 us: shards(): arrived = lax.all_gather(received, 'tp', axis=2, tiled=True)]
    all_to_all x1 -> x0, blocking collectives: 76.5 us -> none  [shards(): lax.all_to_all(outgoing, 'sp', split_axis=1, concat_axis=1, tiled=True)]
    all_to_all x1 -> x0, waiting for transfers between devices: 69.8 us -> none  [shards(): lax.all_to_all(produced.reshape(experts_local, sp_size, tp_size * capacit...]
    all_gather x0 -> x2, blocking collectives: none -> 63.7 us  [the longest x1 32.9 us: experts_by_group(): lax.all_gather(packed, 'sp', axis=0, tiled=True).reshape(-1, block_rows)]
    all_gather x1, waiting for transfers between devices: 14.9 us -> 0.01 us  [shards(): lax.all_gather(attended, 'tp', axis=1, tiled=True)]
    dot_general x3, matrix products: 20 us -> 5.89 us  [the longest x1 3.45 us: experts_by_group(): jnp.einsum('bsr,brg->bsg', slot_hot.reshape(blocks, experts_local * capac...]
    gather x2 -> x0, local copies, waits for them, and re-layouts: 9.69 us -> none  [the longest x1 5.42 us: shards(): picked = result_rows[slot_all.reshape(row_count, picks_count)]]
  transfers between devices with their start and end apart: 8 -> 5, of which waited for: 4 -> 0; matrix products, arithmetic and copies ran while one was open for 4% -> 13% of each run, Pallas kernels for 0% -> 0%
where the time goes in v1:
time: 321 us; the launch traced here: 320 us
  Pallas kernels  151 us (47%)
  blocking collectives  69.7 us (22%)
  local copies, waits for them, and re-layouts  28.5 us (9%)
  other arithmetic  27.6 us (9%)
  matrix products  16.1 us (5%)
  between operations  14.2 us (4%)
  starting transfers between devices  13.1 us (4%)
    pallas_call x1, Pallas kernels, group_experts(): pl.pallas_call(functools.partial(expert_kernel, groups), out_shape=jax.Sh...  151 us
    all_gather x1, blocking collectives, experts_by_group(): lax.all_gather(packed, 'sp', axis=0, tiled=True).reshape(-1, block_rows)  32.9 us
    all_gather x1, blocking collectives, experts_by_group(): routes = lax.all_gather(route_weight.T, 'sp', axis=1, tiled=True)  30.8 us
    ppermute x2, starting transfers between devices, with_halo(): lax.ppermute(lax.slice_in_dim(block, block.shape[dim] - width, None, axis...  10.5 us
    another operation x10, other arithmetic  8.08 us
  transfers between devices with their start and end apart: 5, of which 0 were waited for; matrix products, arithmetic and copies ran while one was open for 13% of the time, Pallas kernels for 0%

profile of v1, /device:TPU:0, one launch (start us, length us, event | category | flops | bytes accessed | tf_op | source)
XLA Modules:
  0.0 320.0 jit_solution(14797162148761921012)
XLA Ops:
  6.5 1.0 constant_dynamic-update-slice_fusion.1
  7.5 1.0 constant_dynamic-update-slice_fusion
  8.5 0.7 fusion.51
  9.1 5.5 %collective-permute-start = (bf16[128,256]{1,0:T(8,128)(2,1)}, bf16[128,256]{1,0:T(8,128)(2,1)}, u32[]{:S(2)}, u32[]{:S(2)}) collective-permute-start(bf16[128,256]{1,0:T(8,128)(2,1)} %get-tuple-element.26), channel_id=1, source_target_pairs={{0,4},{4,8},{8,12},{12,16},{16,20},{20,24},{24,28},{1,5},{5,9},{9,... | collective-permute-start | bytes 196616 | tf_op jit(solution)/shard_map/ppermute | solution.py:25
  14.6 1.3 collective-permute-start.2
  15.9 1.3 fusion.52
  17.2 5.0 %collective-permute-start.1 = (s32[128]{0:T(128)}, s32[128]{0:T(128)}, u32[]{:S(2)}, u32[]{:S(2)}) collective-permute-start(s32[128]{0:T(128)} %get-tuple-element.34), channel_id=1, source_target_pairs={{0,4},{4,8},{8,12},{12,16},{16,20},{20,24},{24,28},{1,5},{5,9},{9,... | collective-permute-start | bytes 1544 | tf_op jit(solution)/shard_map/ppermute | solution.py:25
  22.3 1.3 collective-permute-start.3
  23.6 1.4 fusion.53
  25.0 1.3 slice.131
  26.2 0.8 eq.185
  27.0 0.2 copy.101
  27.3 1.1 and.161
  28.4 1.3 and.162
  29.7 4.8 %reduce-window.20 = s32[4,4,2,128]{3,2,1,0:T(2,128)S(1)} reduce-window(s32[4,4,2,128]{3,2,1,0:T(2,128)S(1)} %reshape.376, s32[]{:T(128)} %constant.112.clone.1), window={size=1x1x1x128 pad=0_0x0_0x0_0x127_0}, to_apply=%region_8.9 | reduce-window | flops 520192 | bytes 32772 | tf_op jit(solution)/shard_map/reduce-window
  34.7 0.1 copy.98
  35.1 0.2 copy.100
  35.3 1.1 eq.189
  36.4 1.8 eq.190
  38.2 0.7 eq.192
  39.3 32.9 %all-gather = s32[8,1,768]{2,1,0:T(1,128)S(1)} all-gather(s32[1,1,768]{2,1,0:T(1,128)S(1)} %reshape.391), channel_id=1, replica_groups=mesh['sp'=8,'tp'=4] {'sp'}, dimensions={0}, use_global_device_ids=true | all-gather | bytes 27648 | tf_op jit(solution)/shard_map/all_gather | solution.py:316
  72.7 2.3 reduce-window.24
  75.0 0.3 slice_reduce_fusion
  75.5 0.6 reduce-window.26
  76.1 0.2 slice_reduce_fusion.1
  76.4 0.6 slice_subtract_fusion
  77.4 0.8 copy.92
  78.3 1.4 bitcast_compare_fusion
  79.7 0.6 pad_add_fusion
  80.4 0.7 and_and_fusion.2
  81.1 0.5 fusion.5
  81.7 1.6 pad_maximum_fusion.3
  83.4 1.0 copy.95
  84.4 1.0 copy.87
  85.5 0.5 fusion.4
  86.2 0.5 fusion.9
  86.7 0.5 fusion.6
  87.3 1.1 fusion.10
  88.5 0.8 convolution_convert_fusion.2
  89.2 0.1 copy-done.7
  89.4 0.7 convolution_convert_fusion.1
  90.1 0.8 convolution_convert_fusion.3
  90.9 0.8 pad_maximum_fusion
  91.7 3.5 %fusion.12 = bf16[32,96,96]{2,1,0:T(8,128)(2,1)S(1)} fusion(pred[32,96,192]{2,1,0:T(32,128)(4,1)S(1)} %copy-done.3, s32[32,192]{1,0:T(8,128)S(1)} %copy-done.8, pred[32,192]{1,0:T(8,128)(4,1)S(1)} %get-tuple-element.16), kind=kOutput, calls=%fused_computation.32 | convolution fusion | flops 114720768 | bytes 1210368 | tf_op jit(solution)/shard_map/bsr,brg->bsg/dot_general | solution.py:331
  95.3 1.6 mul.154
  96.9 1.0 mul.155
  98.2 30.8 %all_gather.11 = f32[2,6144]{1,0:T(2,128)S(1)} all-gather(f32[2,768]{1,0:T(2,128)S(1)} %bitcast.163), channel_id=1, replica_groups=mesh['sp'=8,'tp'=4] {'sp'}, dimensions={1}, use_global_device_ids=true | all-gather | bytes 55296 | tf_op jit(solution)/shard_map/all_gather | solution.py:340
  129.4 0.6 multiply_reduce_fusion.1
  130.3 2.0 copy.108
  132.3 1.7 compare_and_fusion
  134.0 1.3 broadcast_multiply_fusion.1.pick_ref
  135.3 1.9 broadcast_multiply_fusion.join_ref
  137.2 1.1 copy-done.2
  138.3 6.3 %fusion.54 = (f32[768]{0:T(1024)S(1)}, f32[768,2048]{1,0:T(8,128)S(1)}) fusion(bf16[768,1024]{0,1:T(8,128)(2,1)} %all-gather.3.cloned.1.call-done, bf16[1024,2048]{1,0:T(8,128)(2,1)} %param.21, bf16[768,2048]{1,0:T(8,128)(2,1)S(1)} %copy-done.2), kind=kOutput, calls=%fused_computation.141 | convolution fusion | flops 3227516160 | bytes 15207424 | tf_op jit(solution)/shard_map/dot_general | solution.py:436
  144.6 0.8 multiply_reduce_fusion
  145.4 0.9 multiply_convert_fusion
  146.3 1.7 copy-done
  148.0 1.9 convolution_convert_fusion
  149.9 150.7 %shard_map.145 = bf16[4,2,192,512]{3,2,1,0:T(8,128)(2,1)} custom-call(bf16[4,96,2048]{2,1,0:T(8,128)(2,1)} %bitcast.146, bf16[16,192,192]{2,1,0:T(8,128)(2,1)} %broadcast_multiply_fusion.1.pick_ref, bf16[2,16,192,192]{3,2,1,0:T(8,128)(2,1)} %broadcast_multiply_fusion.join_ref, bf16[4,2048,256]{2,1,0:T(8,128)(2,1)} %gate_hbm.1, bf16[4,2048,256]{2,1,0:T(8,128)(2,1)} %up_hbm.1, ...), custom_call_target="tpu_custom_call" | custom-call | tf_op jit(solution)/shard_map/pallas_call | solution.py:265
  300.6 1.5 copy.112
  302.1 0.6 fusion.56
  302.7 1.7 fusion.18
  304.5 6.0 %all-reduce.3 = (f32[768]{0:T(1024)S(1)}, f32[768]{0:T(1024)S(1)}) all-reduce(f32[768]{0:T(1024)S(1)} %get-tuple-element.6, f32[768]{0:T(1024)S(1)} %get-tuple-element.5), channel_id=1, replica_groups=mesh['sp'=8,'tp'=4] {'tp'}, use_global_device_ids=true, to_apply=%region_18.19 | all-reduce | flops 1536 | bytes 12288 | tf_op jit(solution)/shard_map/psum | solution.py:503
  310.5 2.6 multiply_convert_fusion.1
  (121 shorter events, 3.5 us)
Async XLA Ops:
  6.5 130.6 %all-gather.3.cloned.1.call-start = ((), (), s32[]{:S(2)}) async-start(), calls=%async_computation | async-start | bytes 1966080 | tf_op jit(solution)/shard_map/all_gather | solution.py:437
  9.1 72.5 %collective-permute-start = (bf16[128,256]{1,0:T(8,128)(2,1)}, bf16[128,256]{1,0:T(8,128)(2,1)}, u32[]{:S(2)}, u32[]{:S(2)}) collective-permute-start(bf16[128,256]{1,0:T(8,128)(2,1)} %get-tuple-element.26), channel_id=1, source_target_pairs={{0,4},{4,8},{8,12},{12,16},{16,20},{20,24},{24,28},{1,5},{5,9},{9,... | collective-permute-start | bytes 196616 | tf_op jit(solution)/shard_map/ppermute | solution.py:25
  14.6 67.1 %collective-permute-start.2 = (bf16[128,256]{1,0:T(8,128)(2,1)}, bf16[128,256]{1,0:T(8,128)(2,1)}, u32[]{:S(2)}, u32[]{:S(2)}) collective-permute-start(bf16[128,256]{1,0:T(8,128)(2,1)} %get-tuple-element.27), channel_id=1, source_target_pairs={{4,0},{8,4},{12,8},{16,12},{20,16},{24,20},{28,24},{5,1},{9,5},{13... | collective-permute-start | bytes 196616 | tf_op jit(solution)/shard_map/ppermute | solution.py:28
  17.2 62.5 %collective-permute-start.1 = (s32[128]{0:T(128)}, s32[128]{0:T(128)}, u32[]{:S(2)}, u32[]{:S(2)}) collective-permute-start(s32[128]{0:T(128)} %get-tuple-element.34), channel_id=1, source_target_pairs={{0,4},{4,8},{8,12},{12,16},{16,20},{20,24},{24,28},{1,5},{5,9},{9,... | collective-permute-start | bytes 1544 | tf_op jit(solution)/shard_map/ppermute | solution.py:25
  22.3 57.4 %collective-permute-start.3 = (s32[128]{0:T(128)}, s32[128]{0:T(128)}, u32[]{:S(2)}, u32[]{:S(2)}) collective-permute-start(s32[128]{0:T(128)} %get-tuple-element.35), channel_id=1, source_target_pairs={{4,0},{8,4},{12,8},{16,12},{20,16},{24,20},{28,24},{5,1},{9,5},{13... | collective-permute-start | bytes 1544 | tf_op jit(solution)/shard_map/ppermute | solution.py:28
  35.3 3.7 %copy-start.6 = (bf16[768,256]{1,0:T(8,128)(2,1)S(1)}, bf16[768,256]{1,0:T(8,128)(2,1)}, u32[]{:S(2)}) copy-start(bf16[768,256]{1,0:T(8,128)(2,1)} %param.16) | copy-start | bytes 1179652
  36.4 2.7 slice-start
  36.4 2.9 copy-start.14
  36.4 2.9 copy-start.10
  38.2 39.1 %copy-start.22 = (f32[4]{0:T(128)S(1)}, f32[4]{0:T(128)}, u32[]{:S(2)}) copy-start(f32[4]{0:T(128)} %param.20) | copy-start | bytes 52
  38.2 39.2 %slice-start.1 = ((bf16[768,128]{1,0:T(8,128)(2,1)}), bf16[512,128]{1,0:T(8,128)(2,1)S(1)}, s32[]{:S(2)}) async-start(bf16[768,128]{1,0:T(8,128)(2,1)} %param.18), calls=%async_computation.2 | async-start | bytes 262144 | tf_op jit(solution)/shard_map/slice | solution.py:411
  39.1 40.6 %copy-start.9 = (s32[768]{0:T(1024)S(1)}, s32[768]{0:T(1024)}, u32[]{:S(2)}) copy-start(s32[768]{0:T(1024)} %param.19) | copy-start | bytes 9220
  39.1 41.3 %copy-start.12 = (s32[512]{0:T(512)S(1)}, s32[512]{0:T(512)}, u32[]{:S(2)}) copy-start(s32[512]{0:T(512)} %slice.131) | copy-start | bytes 6148
  39.1 41.3 %copy-start.18 = (s32[256]{0:T(256)S(1)}, s32[256]{0:T(256)}, u32[]{:S(2)}) copy-start(s32[256]{0:T(256)} %get-tuple-element.36) | copy-start | bytes 3076
  39.1 41.3 %copy-start.19 = (s32[256]{0:T(256)S(1)}, s32[256]{0:T(256)}, u32[]{:S(2)}) copy-start(s32[256]{0:T(256)} %get-tuple-element.37) | copy-start | bytes 3076
  39.1 41.3 %copy-start.20 = (s32[256]{0:T(256)S(1)}, s32[256]{0:T(256)}, u32[]{:S(2)}) copy-start(s32[256]{0:T(256)} %get-tuple-element.38) | copy-start | bytes 3076
  72.4 7.9 %copy-start.4 = (s32[32,192]{1,0:T(8,128)}, s32[32,192]{1,0:T(8,128)S(1)}, u32[]{:S(2)}) copy-start(s32[32,192]{1,0:T(8,128)S(1)} %get-tuple-element.28) | copy-start | bytes 73732
  72.5 4.6 %copy-start.16 = (s32[4]{0:T(128)}, s32[4]{0:T(128)S(1)}, u32[]{:S(2)}) copy-start(s32[4]{0:T(128)S(1)} %iota_add_fusion.4) | copy-start | bytes 52
  88.5 0.9 copy-start.7
  90.1 1.6 copy-start.3
  90.1 1.6 copy-start.8
  96.8 1.3 copy-start.15
  96.8 32.4 %copy-start.5 = (s32[32,192]{1,0:T(8,128)S(1)}, s32[32,192]{1,0:T(8,128)}, u32[]{:S(2)}) copy-start(s32[32,192]{1,0:T(8,128)} %copy-done.4) | copy-start | bytes 73732
  96.9 32.4 %copy-start.17 = (s32[4]{0:T(128)S(1)}, s32[4]{0:T(128)}, u32[]{:S(2)}) copy-start(s32[4]{0:T(128)} %copy-done.16) | copy-start | bytes 52
  130.3 2.0 copy-start.13
  132.3 3.0 copy-start.1
  135.3 3.0 copy-start.2
  144.6 0.8 copy-start.11
  146.3 1.7 copy-start
  302.1 8.4 %copy-start.21 = (f32[512]{0:T(512)S(1)}, f32[512]{0:T(512)}, u32[]{:S(2)}) copy-start(f32[512]{0:T(512)} %param.29) | copy-start | bytes 6148
Sparse Core Ops, SparseCore 0:
  91.8 19.7 all-gather.2

commit v2 on v1

--- a/solution.py
+++ b/solution.py
@@ -298,6 +298,54 @@
     )(outgoing, picks, joins, gate_weight, up_weight, down_weight)
 
 
+def spread_kernel(count, own_ref, every_ref, held, send_sem, recv_sem):
+    sp = lax.axis_index("sp")
+    tp = lax.axis_index("tp")
+    barrier = pltpu.get_barrier_semaphore()
+    for k in range(1, count):
+        device = (lax.rem(sp + k, count), tp)
+        pl.semaphore_signal(barrier, inc=1, device_id=device, device_id_type=MESH)
+    pl.semaphore_wait(barrier, count - 1)
+
+    def copy(slot, device, k):
+        return pltpu.make_async_remote_copy(
+            src_ref=own_ref,
+            dst_ref=held.at[slot],
+            send_sem=send_sem.at[k],
+            recv_sem=recv_sem.at[k],
+            device_id=device,
+            device_id_type=MESH,
+        )
+
+    copies = [copy(sp, (lax.rem(sp + k, count), tp), k) for k in range(1, count)]
+    for one in copies:
+        one.start()
+    held[sp] = own_ref[...]
+    for k in range(1, count):
+        source = lax.rem(sp + count - k, count)
+        copy(source, (source, tp), k).wait_recv()
+    every_ref[...] = held[...]
+    for one in copies:
+        one.wait_send()
+
+
+def spread(own):
+    count = lax.axis_size("sp")
+    shape = (count,) + own.shape
+    return pl.pallas_call(
+        functools.partial(spread_kernel, count),
+        out_shape=jax.ShapeDtypeStruct(shape, own.dtype),
+        in_specs=[pl.BlockSpec(memory_space=pltpu.VMEM)],
+        out_specs=pl.BlockSpec(memory_space=pltpu.VMEM),
+        scratch_shapes=[
+            pltpu.VMEM(shape, own.dtype),
+            pltpu.SemaphoreType.DMA((count,)),
+            pltpu.SemaphoreType.DMA((count,)),
+        ],
+        compiler_params=pltpu.CompilerParams(collective_id=1, has_side_effects=True),
+    )(own)
+
+
 def group_ranks(mine):
     count = mine.astype(jnp.int32)
     return jnp.cumsum(count, 1) - count
@@ -313,7 +361,9 @@
     groups = experts_local * sp_size // PER_GROUP
     room = capacity * PER_GROUP // member.shape[1]
     packed = (group * PER_GROUP + member[:, 0]) * PER_GROUP + member[:, 1]
-    every = lax.all_gather(packed, "sp", axis=0, tiled=True).reshape(-1, block_rows)
+    facts = jnp.concatenate([packed.astype(jnp.float32)[None], route_weight.T], 0)
+    facts = spread(jnp.pad(facts, ((0, 5), (0, 0))))
+    every = facts[:, 0].astype(jnp.int32).reshape(-1, block_rows)
     own_group = lax.axis_index("sp") * experts_local // PER_GROUP
     first_expert = lax.axis_index("sp") * experts_local % PER_GROUP
     mine = every // (PER_GROUP * PER_GROUP) == own_group
@@ -337,8 +387,7 @@
     pick = pick.reshape(blocks // 2, 2, experts_local, capacity, room).transpose(0, 2, 1, 3, 4)
     both = jnp.eye(2, dtype=jnp.bfloat16)[None, None, :, None, :, None] * pick[:, :, :, :, None, :]
     picks = both.reshape(blocks // 2, experts_local * 2 * capacity, 2 * room)
-    routes = lax.all_gather(route_weight.T, "sp", axis=1, tiled=True)
-    routes = routes.reshape(2, blocks, 1, block_rows)
+    routes = facts[:, 1:3].transpose(1, 0, 2).reshape(2, blocks, 1, block_rows)
     routed = jnp.where(names[0][:, None, :] == local, routes[0], routes[1])
     slot_weight = jnp.sum(slot_hot.astype(jnp.float32) * routed[:, :, None, :], 3)
     slot_weight = slot_weight.reshape(blocks // 2, 2, experts_local, capacity)

time: 321 us -> 264 us (0.82)
  blocking collectives: 69.7 us -> 6.1 us
  Pallas kernels: 151 us -> 155 us
    all_gather x2 -> x0, blocking collectives: 63.7 us -> none  [the longest x1 32.9 us: experts_by_group(): lax.all_gather(packed, 'sp', axis=0, tiled=True).reshape(-1, block_rows)]
    pallas_call x0 -> x1, Pallas kernels: none -> 11.9 us  [spread(): pl.pallas_call(functools.partial(spread_kernel, count), out_shape=jax.Sha...]
    pallas_call x1, Pallas kernels: 151 us -> 143 us  [group_experts(): pl.pallas_call(functools.partial(expert_kernel, groups), out_shape=jax.Sh...]
  transfers between devices with their start and end apart: 5 -> 5, of which waited for: 0 -> 1; matrix products, arithmetic and copies ran while one was open for 13% -> 16% of each run, Pallas kernels for 0% -> 5%
where the time goes in v2:
time: 264 us; the launch traced here: 263 us
  Pallas kernels  155 us (59%)
  other arithmetic  28.3 us (11%)
  local copies, waits for them, and re-layouts  27.2 us (10%)
  matrix products  17.9 us (7%)
  between operations  14.2 us (5%)
  starting transfers between devices  12.6 us (5%)
  blocking collectives  6.1 us (2%)
    pallas_call x1, Pallas kernels, group_experts(): pl.pallas_call(functools.partial(expert_kernel, groups), out_shape=jax.Sh...  143 us
    pallas_call x1, Pallas kernels, spread(): pl.pallas_call(functools.partial(spread_kernel, count), out_shape=jax.Sha...  11.9 us
    ppermute x2, starting transfers between devices, with_halo(): lax.ppermute(lax.slice_in_dim(block, block.shape[dim] - width, None, axis...  10 us
    another operation x10, other arithmetic  8.08 us
    dot_general x1, matrix products, shards(): jnp.dot(lax.all_gather(attended, 'tp', axis=1, tiled=True), weight_rows,...  6.3 us
    psum x1, blocking collectives, shards(): lax.psum((jnp.sum(pre_two, -1), jnp.sum(pre_two * pre_two, -1)), 'tp')  6.1 us
  transfers between devices with their start and end apart: 5, of which 1 were waited for; matrix products, arithmetic and copies ran while one was open for 16% of the time, Pallas kernels for 5%

profile of v2, /device:TPU:0, one launch (start us, length us, event | category | flops | bytes accessed | tf_op | source)
XLA Modules:
  0.0 263.2 jit_solution(9598382117958747230)
XLA Ops:
  6.6 1.0 constant_dynamic-update-slice_fusion.1
  7.6 1.0 constant_dynamic-update-slice_fusion
  8.6 0.7 fusion.51
  9.2 5.5 %collective-permute-start = (bf16[128,256]{1,0:T(8,128)(2,1)}, bf16[128,256]{1,0:T(8,128)(2,1)}, u32[]{:S(2)}, u32[]{:S(2)}) collective-permute-start(bf16[128,256]{1,0:T(8,128)(2,1)} %get-tuple-element.26), channel_id=1, source_target_pairs={{0,4},{4,8},{8,12},{12,16},{16,20},{20,24},{24,28},{1,5},{5,9},{9,... | collective-permute-start | bytes 196616 | tf_op jit(solution)/shard_map/ppermute | solution.py:25
  14.7 1.3 collective-permute-start.2
  16.0 0.8 fusion.52
  16.8 4.5 %collective-permute-start.1 = (s32[128]{0:T(128)S(1)}, s32[128]{0:T(128)S(1)}, u32[]{:S(2)}, u32[]{:S(2)}) collective-permute-start(s32[128]{0:T(128)S(1)} %get-tuple-element.34), channel_id=1, source_target_pairs={{0,4},{4,8},{8,12},{12,16},{16,20},{20,24},{24,28},{1,5},{5,9},{9,... | collective-permute-start | bytes 1544 | tf_op jit(solution)/shard_map/ppermute | solution.py:25
  21.3 1.3 collective-permute-start.3
  22.6 0.8 fusion.53
  23.4 0.7 slice.137
  24.1 0.8 eq.185
  24.9 0.6 fusion.47
  25.5 4.8 %reduce-window.20 = s32[4,4,2,128]{3,2,1,0:T(2,128)S(1)} reduce-window(s32[4,4,2,128]{3,2,1,0:T(2,128)S(1)} %reshape.347, s32[]{:T(128)} %constant.113.clone.1), window={size=1x1x1x128 pad=0_0x0_0x0_0x127_0}, to_apply=%region_8.9 | reduce-window | flops 520192 | bytes 32772 | tf_op jit(solution)/shard_map/reduce-window
  31.1 0.6 select_maximum_fusion.own_ref
  31.7 11.9 %shard_map.145 = f32[8,8,768]{2,1,0:T(8,128)} custom-call(f32[8,768]{1,0:T(8,128)} %select_maximum_fusion.own_ref), custom_call_target="tpu_custom_call" | custom-call | tf_op jit(solution)/shard_map/pallas_call | solution.py:335
  43.6 1.0 convert_reduce_fusion
  44.9 2.3 reduce-window.24
  47.3 0.3 slice_reduce_fusion
  47.9 0.6 reduce-window.26
  48.5 0.2 slice_reduce_fusion.1
  48.8 0.5 bitcast_compare_fusion
  49.4 4.7 %fusion.12 = bf16[32,96,96]{2,1,0:T(8,128)(2,1)} fusion(pred[32,96,192]{2,1,0:T(32,128)(4,1)S(1)} %bitcast_compare_fusion, s32[32,192]{1,0:T(8,128)S(1)} %slice_subtract_fusion, pred[32,192]{1,0:T(8,128)(4,1)S(1)} %get-tuple-element.16), kind=kOutput, calls=%fused_computation.32 | convolution fusion | flops 114720768 | bytes 1210368 | tf_op jit(solution)/shard_map/bsr,brg->bsg/dot_general | solution.py:381
  54.6 0.6 max.46
  55.2 0.8 copy.92
  56.0 0.7 and_and_fusion.2
  56.7 1.1 fusion.5
  57.9 1.6 pad_maximum_fusion.3
  59.5 1.7 copy.94
  61.1 1.0 copy.95
  62.4 0.5 fusion.4
  62.9 0.7 broadcast_maximum_fusion.2
  63.6 0.5 fusion.9
  64.2 0.5 fusion.6
  64.8 1.1 fusion.10
  66.0 0.8 convolution_convert_fusion.2
  66.9 0.8 convolution_convert_fusion.1
  67.6 0.8 convolution_convert_fusion.3
  68.4 0.8 pad_maximum_fusion
  69.2 0.2 copy.101
  69.5 1.1 and.161
  70.6 1.3 and.162
  71.9 0.2 copy.100
  72.1 1.1 eq.189
  73.2 1.8 eq.190
  75.2 1.6 mul.154
  76.8 1.2 mul.155
  78.2 0.9 slice_bitcast_fusion
  79.7 0.6 multiply_reduce_fusion.1
  80.5 1.8 copy.108
  82.3 1.7 compare_and_fusion
  84.0 1.3 broadcast_multiply_fusion.1.pick_ref
  85.3 1.9 broadcast_multiply_fusion.join_ref
  87.2 2.0 all-gather.2.cloned.1.call-done
  89.2 6.3 %fusion.54 = (f32[768]{0:T(1024)S(1)}, f32[768,2048]{1,0:T(8,128)S(1)}) fusion(bf16[768,1024]{0,1:T(8,128)(2,1)} %all-gather.2.cloned.1.call-done, bf16[1024,2048]{1,0:T(8,128)(2,1)} %param.21, bf16[768,2048]{1,0:T(8,128)(2,1)S(1)} %copy-done.2), kind=kOutput, calls=%fused_computation.145 | convolution fusion | flops 3227516160 | bytes 15207424 | tf_op jit(solution)/shard_map/dot_general | solution.py:485
  95.6 0.8 multiply_reduce_fusion
  96.3 0.9 multiply_convert_fusion
  97.2 1.7 copy-done
  98.9 1.9 convolution_convert_fusion
  100.8 143.0 %shard_map.146 = bf16[4,2,192,512]{3,2,1,0:T(8,128)(2,1)} custom-call(bf16[4,96,2048]{2,1,0:T(8,128)(2,1)} %bitcast.148, bf16[16,192,192]{2,1,0:T(8,128)(2,1)} %broadcast_multiply_fusion.1.pick_ref, bf16[2,16,192,192]{3,2,1,0:T(8,128)(2,1)} %broadcast_multiply_fusion.join_ref, bf16[4,2048,256]{2,1,0:T(8,128)(2,1)} %gate_hbm.1, bf16[4,2048,256]{2,1,0:T(8,128)(2,1)} %up_hbm.1, ...), custom_call_target="tpu_custom_call" | custom-call | tf_op jit(solution)/shard_map/pallas_call | solution.py:265
  243.8 1.5 copy.112
  245.3 0.6 fusion.56
  245.9 1.7 fusion.18
  247.6 6.1 %all-reduce.4 = (f32[768]{0:T(1024)S(1)}, f32[768]{0:T(1024)S(1)}) all-reduce(f32[768]{0:T(1024)S(1)} %get-tuple-element.6, f32[768]{0:T(1024)S(1)} %get-tuple-element.5), channel_id=1, replica_groups=mesh['sp'=8,'tp'=4] {'tp'}, use_global_device_ids=true, to_apply=%region_18.19 | all-reduce | flops 1536 | bytes 12288 | tf_op jit(solution)/shard_map/psum | solution.py:552
  253.8 2.6 multiply_convert_fusion.1
  (118 shorter events, 3.7 us)
Async XLA Ops:
  6.5 24.5 %copy-start.12 = (s32[768]{0:T(1024)S(1)}, s32[768]{0:T(1024)}, u32[]{:S(2)}) copy-start(s32[768]{0:T(1024)} %param.23) | copy-start | bytes 9220
  6.5 24.3 %copy-start.6 = (bf16[768,256]{1,0:T(8,128)(2,1)S(1)}, bf16[768,256]{1,0:T(8,128)(2,1)}, u32[]{:S(2)}) copy-start(bf16[768,256]{1,0:T(8,128)(2,1)} %param.16) | copy-start | bytes 1179652
  6.5 24.5 %copy-start.15 = (s32[768,2]{0,1:T(2,128)S(1)}, s32[768,2]{0,1:T(2,128)}, u32[]{:S(2)}) copy-start(s32[768,2]{0,1:T(2,128)} %param.24) | copy-start | bytes 18436
  6.5 24.5 %copy-start.16 = (f32[768,2]{0,1:T(2,128)S(1)}, f32[768,2]{0,1:T(2,128)}, u32[]{:S(2)}) copy-start(f32[768,2]{0,1:T(2,128)} %param.25) | copy-start | bytes 18436
  6.5 82.7 %all-gather.2.cloned.1.call-start = ((), (), s32[]{:S(2)}) async-start(), calls=%async_computation | async-start | bytes 1966080 | tf_op jit(solution)/shard_map/all_gather | solution.py:486
  9.2 48.6 %collective-permute-start = (bf16[128,256]{1,0:T(8,128)(2,1)}, bf16[128,256]{1,0:T(8,128)(2,1)}, u32[]{:S(2)}, u32[]{:S(2)}) collective-permute-start(bf16[128,256]{1,0:T(8,128)(2,1)} %get-tuple-element.26), channel_id=1, source_target_pairs={{0,4},{4,8},{8,12},{12,16},{16,20},{20,24},{24,28},{1,5},{5,9},{9,... | collective-permute-start | bytes 196616 | tf_op jit(solution)/shard_map/ppermute | solution.py:25
  14.7 43.2 %collective-permute-start.2 = (bf16[128,256]{1,0:T(8,128)(2,1)}, bf16[128,256]{1,0:T(8,128)(2,1)}, u32[]{:S(2)}, u32[]{:S(2)}) collective-permute-start(bf16[128,256]{1,0:T(8,128)(2,1)} %get-tuple-element.27), channel_id=1, source_target_pairs={{4,0},{8,4},{12,8},{16,12},{20,16},{24,20},{28,24},{5,1},{9,5},{13... | collective-permute-start | bytes 196616 | tf_op jit(solution)/shard_map/ppermute | solution.py:28
  16.8 39.2 %collective-permute-start.1 = (s32[128]{0:T(128)S(1)}, s32[128]{0:T(128)S(1)}, u32[]{:S(2)}, u32[]{:S(2)}) collective-permute-start(s32[128]{0:T(128)S(1)} %get-tuple-element.34), channel_id=1, source_target_pairs={{0,4},{4,8},{8,12},{12,16},{16,20},{20,24},{24,28},{1,5},{5,9},{9,... | collective-permute-start | bytes 1544 | tf_op jit(solution)/shard_map/ppermute | solution.py:25
  21.3 34.7 %collective-permute-start.3 = (s32[128]{0:T(128)S(1)}, s32[128]{0:T(128)S(1)}, u32[]{:S(2)}, u32[]{:S(2)}) collective-permute-start(s32[128]{0:T(128)S(1)} %get-tuple-element.35), channel_id=1, source_target_pairs={{4,0},{8,4},{12,8},{16,12},{20,16},{24,20},{28,24},{5,1},{9,5},{13... | collective-permute-start | bytes 1544 | tf_op jit(solution)/shard_map/ppermute | solution.py:28
  44.7 9.4 %copy-start.4 = (s32[32,192]{1,0:T(8,128)}, s32[32,192]{1,0:T(8,128)S(1)}, u32[]{:S(2)}) copy-start(s32[32,192]{1,0:T(8,128)S(1)} %get-tuple-element.28) | copy-start | bytes 73732
  44.7 9.4 %copy-start.17 = (s32[4]{0:T(128)}, s32[4]{0:T(128)S(1)}, u32[]{:S(2)}) copy-start(s32[4]{0:T(128)S(1)} %iota_add_fusion.4) | copy-start | bytes 52
  48.8 5.4 %slice-start = ((bf16[768,128]{1,0:T(8,128)(2,1)}), bf16[512,128]{1,0:T(8,128)(2,1)S(1)}, s32[]{:S(2)}) async-start(bf16[768,128]{1,0:T(8,128)(2,1)} %param.17), calls=%async_computation.1 | async-start | bytes 262144 | tf_op jit(solution)/shard_map/slice | solution.py:459
  49.4 5.2 %copy-start.20 = (f32[4]{0:T(128)S(1)}, f32[4]{0:T(128)}, u32[]{:S(2)}) copy-start(f32[4]{0:T(128)} %param.20) | copy-start | bytes 52
  49.4 5.8 %slice-start.1 = ((bf16[768,128]{1,0:T(8,128)(2,1)}), bf16[512,128]{1,0:T(8,128)(2,1)S(1)}, s32[]{:S(2)}) async-start(bf16[768,128]{1,0:T(8,128)(2,1)} %param.18), calls=%async_computation.2 | async-start | bytes 262144 | tf_op jit(solution)/shard_map/slice | solution.py:460
  49.4 6.6 %copy-start.10 = (s32[768]{0:T(1024)S(1)}, s32[768]{0:T(1024)}, u32[]{:S(2)}) copy-start(s32[768]{0:T(1024)} %param.19) | copy-start | bytes 9220
  63.6 1.1 copy-start.9
  63.6 1.1 copy-start.13
  64.8 1.2 copy-start.8
  66.0 0.9 copy-start.7
  67.6 1.6 copy-start.11
  72.1 3.0 %copy-start.3 = (bf16[32,96,96]{2,1,0:T(8,128)(2,1)S(1)}, bf16[32,96,96]{2,1,0:T(8,128)(2,1)}, u32[]{:S(2)}) copy-start(bf16[32,96,96]{2,1,0:T(8,128)(2,1)} %fusion.12) | copy-start | bytes 1769476
  76.8 2.7 %copy-start.5 = (s32[32,192]{1,0:T(8,128)S(1)}, s32[32,192]{1,0:T(8,128)}, u32[]{:S(2)}) copy-start(s32[32,192]{1,0:T(8,128)} %copy-done.4) | copy-start | bytes 73732
  76.8 2.7 %copy-start.18 = (s32[4]{0:T(128)S(1)}, s32[4]{0:T(128)}, u32[]{:S(2)}) copy-start(s32[4]{0:T(128)} %copy-done.17) | copy-start | bytes 52
  82.3 3.0 %copy-start.1 = (bf16[16,192,192]{2,1,0:T(8,128)(2,1)S(1)}, bf16[16,192,192]{2,1,0:T(8,128)(2,1)}, u32[]{:S(2)}) copy-start(bf16[16,192,192]{2,1,0:T(8,128)(2,1)} %copy.108) | copy-start | bytes 3538948
  85.3 3.9 %copy-start.2 = (bf16[768,2048]{1,0:T(8,128)(2,1)S(1)}, bf16[768,2048]{1,0:T(8,128)(2,1)}, u32[]{:S(2)}) copy-start(bf16[768,2048]{1,0:T(8,128)(2,1)} %param.15) | copy-start | bytes 9437188
  95.6 0.8 copy-start.14
  97.2 1.7 copy-start
  245.3 8.5 %copy-start.19 = (f32[512]{0:T(512)S(1)}, f32[512]{0:T(512)}, u32[]{:S(2)}) copy-start(f32[512]{0:T(512)} %param.29) | copy-start | bytes 6148
Sparse Core Ops, SparseCore 0:
  69.3 19.8 all-gather.1
